TPU v7x, 32 devices: a whole 2x2x4 slice. The times are simulated.
32 devices in a mesh: fs: 8 (over z, y), tp: 4 (over x, core).
Axes of the slice: x: 2, y: 2, z: 4, core: 2. Of those that a mesh axis runs over, the one named last changes fastest.
Arguments:
- tokens: bfloat16 [3072, 2048], P(('fs', 'tp')), may hold values from -6 to 6
- ffn1_gain: float32 [2048], replicated, may hold values from 0.1 to 1.9
- ffn1_gate: bfloat16 [2048, 5632], P('fs', 'tp'), may hold values from -0.125 to 0.125
- ffn1_up: bfloat16 [2048, 5632], P('fs', 'tp'), may hold values from -0.125 to 0.125
- ffn1_down: bfloat16 [5632, 2048], P('tp', 'fs'), may hold values from -0.078125 to 0.078125
- mix_gain: float32 [2048], replicated, may hold values from 0.1 to 1.9
- lru_in_weight: bfloat16 [2048, 1536], P('fs', 'tp'), may hold values from -0.125 to 0.125
- lru_gate_weight: bfloat16 [2048, 1536], P('fs', 'tp'), may hold values from -0.125 to 0.125
- conv_weight: bfloat16 [4, 1536], P(None, 'tp'), may hold values from -3 to 3
- gate_a_weight: bfloat16 [24, 64, 64], P('tp'), may hold values from -0.75 to 0.75
- gate_x_weight: bfloat16 [24, 64, 64], P('tp'), may hold values from -0.75 to 0.75
- decay_param: float32 [1536], P('tp'), may hold values from 3.7 to 9
- mix_out_weight: bfloat16 [1536, 2048], P('tp', 'fs'), may hold values from -0.15625 to 0.15625
- ffn2_gain: float32 [2048], replicated, may hold values from 0.1 to 1.9
- ffn2_gate: bfloat16 [2048, 5632], P('fs', 'tp'), may hold values from -0.125 to 0.125
- ffn2_up: bfloat16 [2048, 5632], P('fs', 'tp'), may hold values from -0.125 to 0.125
- ffn2_down: bfloat16 [5632, 2048], P('tp', 'fs'), may hold values from -0.078125 to 0.078125
Outputs:
- layer_out: bfloat16 [3072, 2048], P(('fs', 'tp'))
All inputs are finite; a program needn't handle non-finite values.
Results may differ from a plain program's by a relative error of at most 0.017.
Values may be sent and summed in bfloat16 or wider, within the bound.
A program may use at most 64 MiB of HBM per device.

v0:
```python
import jax
import jax.numpy as jnp
from jax import lax
from jax.sharding import PartitionSpec as P

EPS = 1e-06


def rms_rows(values, gain):
    wide = values.astype(jnp.float32)
    scale = lax.rsqrt(jnp.mean(wide * wide, axis=-1, keepdims=True) + EPS)
    return (wide * scale * gain).astype(jnp.bfloat16)


def gather_rows(values):
    return lax.all_gather(values, "tp", axis=0, tiled=True)


def pair_step(rows, pieces):
    return (
        jnp.dot(rows, pieces[0], preferred_element_type=jnp.float32),
        jnp.dot(rows, pieces[1], preferred_element_type=jnp.float32),
    )


def block_hidden(rows, gate_weight, up_weight):
    gate, upper = pair_step(
        rows,
        (
            lax.all_gather(gate_weight, "fs", axis=0, tiled=True),
            lax.all_gather(up_weight, "fs", axis=0, tiled=True),
        ),
    )
    return (jax.nn.silu(gate) * upper).astype(jnp.bfloat16)


def block_terms(hidden, down_weight):
    return jnp.dot(
        hidden,
        lax.all_gather(down_weight, "fs", axis=1, tiled=True),
        preferred_element_type=jnp.float32,
    )


def reduce_rows(terms):
    return lax.psum_scatter(
        terms.astype(jnp.bfloat16), "tp", scatter_dimension=0, tiled=True
    ).astype(jnp.float32)


def whole_sum(terms):
    return lax.psum(terms.astype(jnp.bfloat16), "tp").astype(jnp.float32)


def combine(earlier, later):
    return (earlier[0] * later[0], later[0] * earlier[1] + later[1])


def mixer_terms(
    rows,
    lru_in_weight,
    lru_gate_weight,
    conv_weight,
    gate_a_weight,
    gate_x_weight,
    decay_param,
    mix_out_weight,
):
    lru_x, lru_gate = pair_step(
        rows,
        (
            lax.all_gather(lru_in_weight, "fs", axis=0, tiled=True),
            lax.all_gather(lru_gate_weight, "fs", axis=0, tiled=True),
        ),
    )
    lru_low = lru_x.astype(jnp.bfloat16).astype(jnp.float32)
    gate_low = lru_gate.astype(jnp.bfloat16).astype(jnp.float32)
    length = rows.shape[0]
    taps_count = conv_weight.shape[0]
    padded = jnp.pad(lru_low, ((taps_count - 1, 0), (0, 0)))
    taps = conv_weight.astype(jnp.float32)
    conv = jnp.zeros_like(lru_low)
    for offset in range(taps_count):
        conv = (
            conv + taps[offset] * padded[taps_count - 1 - offset : taps_count - 1 - offset + length]
        )
    conv_low = conv.astype(jnp.bfloat16)
    blocks = conv_low.reshape(length, gate_a_weight.shape[0], gate_a_weight.shape[1])
    recall = jax.nn.sigmoid(
        jnp.einsum(
            "sbi,bij->sbj", blocks, gate_a_weight, preferred_element_type=jnp.float32
        ).reshape(length, -1)
    )
    admit = jax.nn.sigmoid(
        jnp.einsum(
            "sbi,bij->sbj", blocks, gate_x_weight, preferred_element_type=jnp.float32
        ).reshape(length, -1)
    )
    log_keep = -8.0 * recall * jax.nn.softplus(-decay_param)
    drive = jnp.sqrt(-jnp.expm1(2.0 * log_keep)) * admit * conv_low.astype(jnp.float32)
    _, state = lax.associative_scan(combine, (jnp.exp(log_keep), drive), axis=0)
    mixed = (state * jax.nn.gelu(gate_low)).astype(jnp.bfloat16)
    return jnp.dot(
        mixed,
        lax.all_gather(mix_out_weight, "fs", axis=1, tiled=True),
        preferred_element_type=jnp.float32,
    )


def body(
    tokens,
    ffn1_gain,
    ffn1_gate,
    ffn1_up,
    ffn1_down,
    mix_gain,
    lru_in_weight,
    lru_gate_weight,
    conv_weight,
    gate_a_weight,
    gate_x_weight,
    decay_param,
    mix_out_weight,
    ffn2_gain,
    ffn2_gate,
    ffn2_up,
    ffn2_down,
):
    local = tokens.shape[0]
    whole = gather_rows(tokens)
    terms = block_terms(block_hidden(rms_rows(whole, ffn1_gain), ffn1_gate, ffn1_up), ffn1_down)
    first = (whole.astype(jnp.float32) + 0.5 * whole_sum(terms)).astype(jnp.bfloat16)
    terms = mixer_terms(
        rms_rows(first, mix_gain),
        lru_in_weight,
        lru_gate_weight,
        conv_weight,
        gate_a_weight,
        gate_x_weight,
        decay_param,
        mix_out_weight,
    )
    second_all = (first.astype(jnp.float32) + whole_sum(terms)).astype(jnp.bfloat16)
    rows = rms_rows(second_all, ffn2_gain)
    second = lax.dynamic_slice_in_dim(second_all, lax.axis_index("tp") * local, local, 0)
    terms = block_terms(block_hidden(rows, ffn2_gate, ffn2_up), ffn2_down)
    return (second.astype(jnp.float32) + 0.5 * reduce_rows(terms)).astype(jnp.bfloat16)


def solution(mesh):
    in_specs = (
        P(("fs", "tp"), None),
        P(),
        P("fs", "tp"),
        P("fs", "tp"),
        P("tp", "fs"),
        P(),
        P("fs", "tp"),
        P("fs", "tp"),
        P(None, "tp"),
        P("tp", None, None),
        P("tp", None, None),
        P("tp"),
        P("tp", "fs"),
        P(),
        P("fs", "tp"),
        P("fs", "tp"),
        P("tp", "fs"),
    )
    out_specs = P(("fs", "tp"), None)
    return jax.shard_map(body, mesh=mesh, in_specs=in_specs, out_specs=out_specs, check_vma=False)
```

profile of v0, /device:TPU:0, one launch (start us, length us, event | category | flops | bytes accessed | tf_op | source)
XLA Modules:
  0.0 873.1 jit_solution(14798320163815893249)
XLA Ops:
  9.4 21.9 %all-gather.11.cloned.1.call-done = bf16[384,2048]{1,0:T(8,128)(2,1)} async-done(((bf16[96,2048]{1,0:T(8,128)(2,1)}), bf16[384,2048]{1,0:T(8,128)(2,1)}) %all-gather.11.cloned.1.call-update) | async-done | bytes 1572880 | tf_op jit(solution)/shard_map/all_gather | solution.py:16
  31.3 1.8 fusion.3
  33.1 92.7 %all-gather.13.cloned.1.call-done = bf16[2048,1408]{1,0:T(8,128)(2,1)} async-done(((bf16[256,1408]{1,0:T(8,128)(2,1)}), bf16[2048,1408]{1,0:T(8,128)(2,1)}) %all-gather.13.cloned.1.call-update) | async-done | bytes 5767184 | tf_op jit(solution)/shard_map/all_gather | solution.py:30
  125.8 7.1 fusion.33
  132.9 85.6 %all-gather.15.cloned.1.call-done = bf16[2048,1408]{1,0:T(8,128)(2,1)} async-done(((bf16[256,1408]{1,0:T(8,128)(2,1)}), bf16[2048,1408]{1,0:T(8,128)(2,1)}) %all-gather.15.cloned.1.call-update) | async-done | bytes 5767184 | tf_op jit(solution)/shard_map/all_gather | solution.py:31
  218.5 93.2 %all-gather.17.cloned.1.call-done = bf16[1408,2048]{1,0:T(8,128)(2,1)} async-done(((bf16[1408,256]{1,0:T(8,128)(2,1)}), bf16[1408,2048]{1,0:T(8,128)(2,1)}) %all-gather.17.cloned.1.call-update) | async-done | bytes 5767184 | tf_op jit(solution)/shard_map/all_gather | solution.py:40
  311.8 11.3 %convolution_convert_fusion.2 = bf16[384,2048]{1,0:T(8,128)(2,1)} fusion(bf16[1408,2048]{1,0:T(8,128)(2,1)} %all-gather.17.cloned.1.call-done, bf16[2048,1408]{1,0:T(8,128)(2,1)} %all-gather.15.cloned.1.call-done, f32[384,1408]{1,0:T(8,128)} %fusion.33, bf16[384,2048]{1,0:T(8,128)(2,1)S(1)} %copy-done.2, f32[2048]{0:T(1024)S(1)} %copy-done.16, ...), kind=kOutput, calls=%fused_computation.25 | convolution fusion | flops 4436361216 | bytes 16852480 | tf_op jit(solution)/shard_map/dot_general | solution.py:38
  325.5 38.8 %all-reduce.20.cloned.1.call-done = bf16[384,2048]{1,0:T(8,128)(2,1)} async-done(((bf16[384,2048]{1,0:T(8,128)(2,1)}), bf16[384,2048]{1,0:T(8,128)(2,1)}) %all-reduce.20.cloned.1.call-update) | async-done | bytes 1572880 | tf_op jit(solution)/shard_map/psum | solution.py:52
  364.3 2.3 fusion.7
  366.5 44.0 %all-gather.19.cloned.1.call-done = bf16[2048,384]{1,0:T(8,128)(2,1)} async-done(((bf16[256,384]{1,0:T(8,128)(2,1)}), bf16[2048,384]{1,0:T(8,128)(2,1)}) %all-gather.19.cloned.1.call-update) | async-done | bytes 1572880 | tf_op jit(solution)/shard_map/all_gather | solution.py:72
  410.6 2.4 fusion.20
  416.4 1.9 multiply_exponential_fusion
  428.0 1.9 fusion.65
  482.3 17.9 %all-gather.23.cloned.1.call-done = bf16[384,2048]{1,0:T(8,128)(2,1)} async-done(((bf16[384,256]{1,0:T(8,128)(2,1)}), bf16[384,2048]{1,0:T(8,128)(2,1)}) %all-gather.23.cloned.1.call-update) | async-done | bytes 1572880 | tf_op jit(solution)/shard_map/all_gather | solution.py:105
  500.2 5.3 convolution_convert_fusion.1
  507.7 39.0 %all-reduce.22.cloned.1.call-done = bf16[384,2048]{1,0:T(8,128)(2,1)} async-done(((bf16[384,2048]{1,0:T(8,128)(2,1)}), bf16[384,2048]{1,0:T(8,128)(2,1)}) %all-reduce.22.cloned.1.call-update) | async-done | bytes 1572880 | tf_op jit(solution)/shard_map/psum | solution.py:52
  546.7 2.1 fusion
  548.8 92.3 %all-gather.25.cloned.1.call-done = bf16[2048,1408]{1,0:T(8,128)(2,1)} async-done(((bf16[256,1408]{1,0:T(8,128)(2,1)}), bf16[2048,1408]{1,0:T(8,128)(2,1)}) %all-gather.25.cloned.1.call-update) | async-done | bytes 5767184 | tf_op jit(solution)/shard_map/all_gather | solution.py:30
  641.1 6.6 fusion.37
  647.7 86.1 %all-gather.27.cloned.1.call-done = bf16[2048,1408]{1,0:T(8,128)(2,1)} async-done(((bf16[256,1408]{1,0:T(8,128)(2,1)}), bf16[2048,1408]{1,0:T(8,128)(2,1)}) %all-gather.27.cloned.1.call-update) | async-done | bytes 5767184 | tf_op jit(solution)/shard_map/all_gather | solution.py:31
  733.8 93.2 %all-gather.29.cloned.1.call-done = bf16[1408,2048]{1,0:T(8,128)(2,1)} async-done(((bf16[1408,256]{1,0:T(8,128)(2,1)}), bf16[1408,2048]{1,0:T(8,128)(2,1)}) %all-gather.29.cloned.1.call-update) | async-done | bytes 5767184 | tf_op jit(solution)/shard_map/all_gather | solution.py:40
  827.1 11.3 %convolution_convert_fusion = bf16[384,2048]{1,0:T(8,128)(2,1)} fusion(bf16[1408,2048]{1,0:T(8,128)(2,1)} %all-gather.29.cloned.1.call-done, bf16[2048,1408]{1,0:T(8,128)(2,1)} %all-gather.27.cloned.1.call-done, f32[384,1408]{1,0:T(8,128)} %fusion.37, bf16[384,2048]{1,0:T(8,128)(2,1)S(1)} %get-tuple-element.10, f32[2048]{0:T(1024)S(1)} %copy-done.19, ...), kind=kOutput, calls=%fused_computation.23 | convolution fusion | flops 4436361216 | bytes 16852480 | tf_op jit(solution)/shard_map/dot_general | solution.py:38
  838.4 26.3 %reduce-scatter.2.cloned.1.call-done = bf16[96,2048]{1,0:T(8,128)(2,1)} async-done(((bf16[384,2048]{1,0:T(8,128)(2,1)}), bf16[96,2048]{1,0:T(8,128)(2,1)}) %reduce-scatter.2.cloned.1.call-update) | async-done | bytes 393232 | tf_op jit(solution)/shard_map/reduce_scatter | solution.py:46
  864.7 1.9 add_convert_fusion
  (172 shorter events, 72.4 us)
Async XLA Ops:
  6.5 407.0 %copy-start = (bf16[6,64,64]{2,1,0:T(8,128)(2,1)S(1)}, bf16[6,64,64]{2,1,0:T(8,128)(2,1)}, u32[]{:S(2)}) copy-start(bf16[6,64,64]{2,1,0:T(8,128)(2,1)} %param.26) | copy-start | bytes 147460
  6.5 119.3 %copy-start.16 = (f32[2048]{0:T(1024)S(1)}, f32[2048]{0:T(1024)}, u32[]{:S(2)}) copy-start(f32[2048]{0:T(1024)} %param.18) | copy-start | bytes 24580
  6.5 24.7 %all-gather.11.cloned.1.call-start = ((), (), s32[]{:S(2)}) async-start(), calls=%async_computation.1 | async-start | bytes 1966080 | tf_op jit(solution)/shard_map/all_gather | solution.py:16
  7.3 118.5 %all-gather.13.cloned.1.call-start = ((), (), s32[]{:S(2)}) async-start(), calls=%async_computation.2 | async-start | bytes 6488064 | tf_op jit(solution)/shard_map/all_gather | solution.py:30
  8.0 210.5 %all-gather.15.cloned.1.call-start = ((), (), s32[]{:S(2)}) async-start(), calls=%async_computation.3 | async-start | bytes 6488064 | tf_op jit(solution)/shard_map/all_gather | solution.py:31
  8.7 303.0 %all-gather.17.cloned.1.call-start = ((), (), s32[]{:S(2)}) async-start(), calls=%async_computation.4 | async-start | bytes 6488064 | tf_op jit(solution)/shard_map/all_gather | solution.py:40
  9.3 354.9 %all-reduce.20.cloned.1.call-start = ((), (), s32[]{:S(2)}) async-start(), calls=%async_computation.5 | async-start | bytes 3145728 | tf_op jit(solution)/shard_map/psum | solution.py:52
  33.1 278.7 %copy-start.2 = (bf16[384,2048]{1,0:T(8,128)(2,1)S(1)}, bf16[384,2048]{1,0:T(8,128)(2,1)}, u32[]{:S(2)}) copy-start(bf16[384,2048]{1,0:T(8,128)(2,1)} %all-gather.11.cloned.1.call-done) | copy-start | bytes 4718596
  323.1 87.5 %all-gather.19.cloned.1.call-start = ((), (), s32[]{:S(2)}) async-start(), calls=%async_computation.6 | async-start | bytes 1769472 | tf_op jit(solution)/shard_map/all_gather | solution.py:72
  323.6 158.6 %all-gather.21.cloned.1.call-start = ((), (), s32[]{:S(2)}) async-start(), calls=%async_computation.7 | async-start | bytes 1769472 | tf_op jit(solution)/shard_map/all_gather | solution.py:73
  324.4 175.8 %all-gather.23.cloned.1.call-start = ((), (), s32[]{:S(2)}) async-start(), calls=%async_computation.8 | async-start | bytes 1769472 | tf_op jit(solution)/shard_map/all_gather | solution.py:105
  325.1 221.5 %all-reduce.22.cloned.1.call-start = ((), (), s32[]{:S(2)}) async-start(), calls=%async_computation.9 | async-start | bytes 3145728 | tf_op jit(solution)/shard_map/psum | solution.py:52
  325.5 85.1 %copy-start.17 = (f32[2048]{0:T(1024)S(1)}, f32[2048]{0:T(1024)}, u32[]{:S(2)}) copy-start(f32[2048]{0:T(1024)} %param.22) | copy-start | bytes 24580
  366.5 46.5 %copy-start.13 = (f32[384]{0:T(512)}, f32[384]{0:T(512)S(1)}, u32[]{:S(2)}) copy-start(f32[384]{0:T(512)S(1)} %add_rsqrt_fusion.1) | copy-start | bytes 4612
  462.7 12.0 %copy-start.5 = (f32[5,384]{1,0:T(8,128)S(1)}, f32[5,384]{1,0:T(8,128)}, u32[]{:S(2)}) copy-start(f32[5,384]{1,0:T(8,128)} %slice.249) | copy-start | bytes 23044
  462.7 12.1 %copy-start.6 = (f32[5,384]{1,0:T(8,128)S(1)}, f32[5,384]{1,0:T(8,128)}, u32[]{:S(2)}) copy-start(f32[5,384]{1,0:T(8,128)} %slice.268) | copy-start | bytes 23044
  480.3 19.9 %copy-start.14 = (f32[384]{0:T(512)S(1)}, f32[384]{0:T(512)}, u32[]{:S(2)}) copy-start(f32[384]{0:T(512)} %copy-done.13) | copy-start | bytes 4612
  480.3 19.9 %copy-start.18 = (f32[2048]{0:T(1024)S(1)}, f32[2048]{0:T(1024)}, u32[]{:S(2)}) copy-start(f32[2048]{0:T(1024)} %param.22) | copy-start | bytes 24580
  505.5 135.6 %all-gather.25.cloned.1.call-start = ((), (), s32[]{:S(2)}) async-start(), calls=%async_computation.10 | async-start | bytes 6488064 | tf_op jit(solution)/shard_map/all_gather | solution.py:30
  506.1 227.8 %all-gather.27.cloned.1.call-start = ((), (), s32[]{:S(2)}) async-start(), calls=%async_computation.11 | async-start | bytes 6488064 | tf_op jit(solution)/shard_map/all_gather | solution.py:31
  506.8 320.3 %all-gather.29.cloned.1.call-start = ((), (), s32[]{:S(2)}) async-start(), calls=%async_computation.12 | async-start | bytes 6488064 | tf_op jit(solution)/shard_map/all_gather | solution.py:40
  507.4 133.7 %copy-start.19 = (f32[2048]{0:T(1024)S(1)}, f32[2048]{0:T(1024)}, u32[]{:S(2)}) copy-start(f32[2048]{0:T(1024)} %param.30) | copy-start | bytes 24580
  507.4 357.3 %reduce-scatter.2.cloned.1.call-start = ((), (), s32[]{:S(2)}) async-start(), calls=%async_computation.13 | async-start | bytes 1966080 | tf_op jit(solution)/shard_map/reduce_scatter | solution.py:46
  827.1 39.5 %copy-start.1 = (bf16[6,64,64]{2,1,0:T(8,128)(2,1)S(1)}, bf16[6,64,64]{2,1,0:T(8,128)(2,1)}, u32[]{:S(2)}) copy-start(bf16[6,64,64]{2,1,0:T(8,128)(2,1)} %param.26) | copy-start | bytes 147460
  (9 other events, 46.1 us)
Sparse Core Ops, SparseCore 0:
  8.9 22.3 all-gather.10
  33.5 92.3 all-gather.12
  128.0 90.4 all-gather.14
  220.4 91.2 all-gather.16
  323.2 41.0 all-reduce.19
  366.3 44.2 all-gather.18
  412.8 42.5 all-gather.20
  457.4 42.7 all-gather.22
  505.6 41.0 all-reduce.21
  548.7 92.3 all-gather.24
  643.3 90.4 all-gather.26
  735.7 91.2 all-gather.28
  838.5 26.1 reduce-scatter.1
where the time goes:
time: 875 us; the launch traced here: 873 us
  waiting for transfers between devices  737 us (84%)
  local copies, waits for them, and re-layouts  51.5 us (6%)
  matrix products  44.7 us (5%)
  other arithmetic  24.8 us (3%)
  between operations  13.8 us (2%)
    all_gather x2, waiting for transfers between devices, block_terms(): lax.all_gather(down_weight, 'fs', axis=1, tiled=True)  186 us
    all_gather x2, waiting for transfers between devices, block_hidden(): lax.all_gather(gate_weight, 'fs', axis=0, tiled=True)  185 us
    all_gather x2, waiting for transfers between devices, block_hidden(): lax.all_gather(up_weight, 'fs', axis=0, tiled=True)  172 us
    psum x2, waiting for transfers between devices, whole_sum(): return lax.psum(terms.astype(jnp.bfloat16), 'tp').astype(jnp.float32)  77.8 us
    slice x49, local copies, waits for them, and re-layouts, mixer_terms(): _, state = lax.associative_scan(combine, (jnp.exp(log_keep), drive), axis=0)  47 us
    all_gather x1, waiting for transfers between devices, mixer_terms(): lax.all_gather(lru_in_weight, 'fs', axis=0, tiled=True)  44 us
    reduce_scatter x1, waiting for transfers between devices, reduce_rows(): lax.psum_scatter(terms.astype(jnp.bfloat16), 'tp', scatter_dimension=0, t...  26.3 us
    dot_general x2, matrix products, block_terms(): jnp.dot(hidden, lax.all_gather(down_weight, 'fs', axis=1, tiled=True), pr...  22.6 us
  transfers between devices with their start and end apart: 13, of which 12 were waited for; matrix products, arithmetic and copies ran while one was open for 10% of the time, Pallas kernels for 0%

commit v1 on v0

--- a/solution.py
+++ b/solution.py
@@ -49,7 +49,7 @@
 
 
 def whole_sum(terms):
-    return lax.psum(terms.astype(jnp.bfloat16), "tp").astype(jnp.float32)
+    return jnp.sum(lax.all_gather(terms.astype(jnp.bfloat16), "tp"), axis=0).astype(jnp.float32)
 
 
 def combine(earlier, later):

time: 875 us -> 882 us (level)
  other arithmetic: 24.8 us -> 34.6 us
    all_gather x0 -> x2, waiting for transfers between devices: none -> 84.8 us  [whole_sum(): lax.all_gather(terms.astype(jnp.bfloat16), 'tp')]
    psum x2 -> x0, waiting for transfers between devices: 77.8 us -> none  [whole_sum(): return lax.psum(terms.astype(jnp.bfloat16), 'tp').astype(jnp.float32)]
    reduce_sum x0 -> x2, other arithmetic: none -> 9.94 us  [whole_sum(): jnp.sum(lax.all_gather(terms.astype(jnp.bfloat16), 'tp'), axis=0)]
  transfers between devices with their start and end apart: 13 -> 13, of which waited for: 12 -> 12; matrix products, arithmetic and copies ran while one was open for 10% -> 12% of each run, Pallas kernels for 0% -> 0%
where the time goes in v1:
time: 882 us; the launch traced here: 880 us
  waiting for transfers between devices  734 us (83%)
  local copies, waits for them, and re-layouts  51.6 us (6%)
  matrix products  45.4 us (5%)
  other arithmetic  34.6 us (4%)
  between operations  13.8 us (2%)
    all_gather x2, waiting for transfers between devices, block_terms(): lax.all_gather(down_weight, 'fs', axis=1, tiled=True)  186 us
    all_gather x2, waiting for transfers between devices, block_hidden(): lax.all_gather(gate_weight, 'fs', axis=0, tiled=True)  181 us
    all_gather x2, waiting for transfers between devices, block_hidden(): lax.all_gather(up_weight, 'fs', axis=0, tiled=True)  171 us
    all_gather x2, waiting for transfers between devices, whole_sum(): lax.all_gather(terms.astype(jnp.bfloat16), 'tp')  84.8 us
    slice x49, local copies, waits for them, and re-layouts, mixer_terms(): _, state = lax.associative_scan(combine, (jnp.exp(log_keep), drive), axis=0)  47 us
    all_gather x1, waiting for transfers between devices, mixer_terms(): lax.all_gather(lru_in_weight, 'fs', axis=0, tiled=True)  38.2 us
    reduce_scatter x1, waiting for transfers between devices, reduce_rows(): lax.psum_scatter(terms.astype(jnp.bfloat16), 'tp', scatter_dimension=0, t...  26.3 us
    dot_general x2, matrix products, block_terms(): jnp.dot(hidden, lax.all_gather(down_weight, 'fs', axis=1, tiled=True), pr...  22.5 us
  transfers between devices with their start and end apart: 13, of which 12 were waited for; matrix products, arithmetic and copies ran while one was open for 12% of the time, Pallas kernels for 0%

profile of v1, /device:TPU:0, one launch (start us, length us, event | category | flops | bytes accessed | tf_op | source)
XLA Modules:
  0.0 880.1 jit_solution(17935002308620244880)
XLA Ops:
  9.4 21.9 %all-gather.15.cloned.1.call-done = bf16[384,2048]{1,0:T(8,128)(2,1)} async-done(((bf16[96,2048]{1,0:T(8,128)(2,1)}), bf16[384,2048]{1,0:T(8,128)(2,1)}) %all-gather.15.cloned.1.call-update) | async-done | bytes 1572880 | tf_op jit(solution)/shard_map/all_gather | solution.py:16
  33.1 92.7 %all-gather.17.cloned.1.call-done = bf16[2048,1408]{1,0:T(8,128)(2,1)} async-done(((bf16[256,1408]{1,0:T(8,128)(2,1)}), bf16[2048,1408]{1,0:T(8,128)(2,1)}) %all-gather.17.cloned.1.call-update) | async-done | bytes 5767184 | tf_op jit(solution)/shard_map/all_gather | solution.py:30
  125.8 7.1 fusion.33
  132.9 85.6 %all-gather.19.cloned.1.call-done = bf16[2048,1408]{1,0:T(8,128)(2,1)} async-done(((bf16[256,1408]{1,0:T(8,128)(2,1)}), bf16[2048,1408]{1,0:T(8,128)(2,1)}) %all-gather.19.cloned.1.call-update) | async-done | bytes 5767184 | tf_op jit(solution)/shard_map/all_gather | solution.py:31
  218.5 93.2 %all-gather.21.cloned.1.call-done = bf16[1408,2048]{1,0:T(8,128)(2,1)} async-done(((bf16[1408,256]{1,0:T(8,128)(2,1)}), bf16[1408,2048]{1,0:T(8,128)(2,1)}) %all-gather.21.cloned.1.call-update) | async-done | bytes 5767184 | tf_op jit(solution)/shard_map/all_gather | solution.py:40
  311.8 11.3 %convolution_convert_fusion.2 = bf16[384,2048]{1,0:T(8,128)(2,1)} fusion(bf16[1408,2048]{1,0:T(8,128)(2,1)} %all-gather.21.cloned.1.call-done, bf16[2048,1408]{1,0:T(8,128)(2,1)} %all-gather.19.cloned.1.call-done, f32[384,1408]{1,0:T(8,128)} %fusion.33, bf16[384,2048]{1,0:T(8,128)(2,1)S(1)} %copy-done.2, f32[2048]{0:T(1024)S(1)} %copy-done.17, ...), kind=kOutput, calls=%fused_computation.25 | convolution fusion | flops 4436361216 | bytes 16852480 | tf_op jit(solution)/shard_map/dot_general | solution.py:38
  325.5 42.3 %all-gather.35.cloned.1.call-done = bf16[1536,2048]{1,0:T(8,128)(2,1)} async-done(((bf16[384,2048]{1,0:T(8,128)(2,1)}), bf16[1536,2048]{1,0:T(8,128)(2,1)}) %all-gather.35.cloned.1.call-update) | async-done | bytes 6291472 | tf_op jit(solution)/shard_map/all_gather | solution.py:52
  367.8 5.7 reduce_sum.52
  373.5 2.3 fusion.7
  375.8 38.2 %all-gather.23.cloned.1.call-done = bf16[2048,384]{1,0:T(8,128)(2,1)} async-done(((bf16[256,384]{1,0:T(8,128)(2,1)}), bf16[2048,384]{1,0:T(8,128)(2,1)}) %all-gather.23.cloned.1.call-update) | async-done | bytes 1572880 | tf_op jit(solution)/shard_map/all_gather | solution.py:72
  414.0 2.4 fusion.20
  419.9 1.9 multiply_exponential_fusion
  431.5 1.9 fusion.65
  485.9 17.8 %all-gather.27.cloned.1.call-done = bf16[384,2048]{1,0:T(8,128)(2,1)} async-done(((bf16[384,256]{1,0:T(8,128)(2,1)}), bf16[384,2048]{1,0:T(8,128)(2,1)}) %all-gather.27.cloned.1.call-update) | async-done | bytes 1572880 | tf_op jit(solution)/shard_map/all_gather | solution.py:105
  503.7 5.3 convolution_convert_fusion.1
  511.2 42.5 %all-gather.37.cloned.1.call-done = bf16[1536,2048]{1,0:T(8,128)(2,1)} async-done(((bf16[384,2048]{1,0:T(8,128)(2,1)}), bf16[1536,2048]{1,0:T(8,128)(2,1)}) %all-gather.37.cloned.1.call-update) | async-done | bytes 6291472 | tf_op jit(solution)/shard_map/all_gather | solution.py:52
  553.8 4.2 reduce_sum.54
  558.0 1.9 fusion
  559.9 88.3 %all-gather.29.cloned.1.call-done = bf16[2048,1408]{1,0:T(8,128)(2,1)} async-done(((bf16[256,1408]{1,0:T(8,128)(2,1)}), bf16[2048,1408]{1,0:T(8,128)(2,1)}) %all-gather.29.cloned.1.call-update) | async-done | bytes 5767184 | tf_op jit(solution)/shard_map/all_gather | solution.py:30
  648.1 7.2 fusion.37
  655.4 85.5 %all-gather.31.cloned.1.call-done = bf16[2048,1408]{1,0:T(8,128)(2,1)} async-done(((bf16[256,1408]{1,0:T(8,128)(2,1)}), bf16[2048,1408]{1,0:T(8,128)(2,1)}) %all-gather.31.cloned.1.call-update) | async-done | bytes 5767184 | tf_op jit(solution)/shard_map/all_gather | solution.py:31
  740.9 93.2 %all-gather.33.cloned.1.call-done = bf16[1408,2048]{1,0:T(8,128)(2,1)} async-done(((bf16[1408,256]{1,0:T(8,128)(2,1)}), bf16[1408,2048]{1,0:T(8,128)(2,1)}) %all-gather.33.cloned.1.call-update) | async-done | bytes 5767184 | tf_op jit(solution)/shard_map/all_gather | solution.py:40
  834.1 11.2 %convolution_convert_fusion = bf16[384,2048]{1,0:T(8,128)(2,1)} fusion(bf16[1408,2048]{1,0:T(8,128)(2,1)} %all-gather.33.cloned.1.call-done, bf16[2048,1408]{1,0:T(8,128)(2,1)} %all-gather.31.cloned.1.call-done, f32[384,1408]{1,0:T(8,128)} %fusion.37, bf16[384,2048]{1,0:T(8,128)(2,1)S(1)} %copy-done.3, f32[2048]{0:T(1024)S(1)} %copy-done.20, ...), kind=kOutput, calls=%fused_computation.23 | convolution fusion | flops 4436361216 | bytes 16852480 | tf_op jit(solution)/shard_map/dot_general | solution.py:38
  845.4 26.3 %reduce-scatter.2.cloned.1.call-done = bf16[96,2048]{1,0:T(8,128)(2,1)} async-done(((bf16[384,2048]{1,0:T(8,128)(2,1)}), bf16[96,2048]{1,0:T(8,128)(2,1)}) %reduce-scatter.2.cloned.1.call-update) | async-done | bytes 393232 | tf_op jit(solution)/shard_map/reduce_scatter | solution.py:46
  (176 shorter events, 76.2 us)
Async XLA Ops:
  6.5 410.5 %copy-start = (bf16[6,64,64]{2,1,0:T(8,128)(2,1)S(1)}, bf16[6,64,64]{2,1,0:T(8,128)(2,1)}, u32[]{:S(2)}) copy-start(bf16[6,64,64]{2,1,0:T(8,128)(2,1)} %param.26) | copy-start | bytes 147460
  6.5 119.3 %copy-start.17 = (f32[2048]{0:T(1024)S(1)}, f32[2048]{0:T(1024)}, u32[]{:S(2)}) copy-start(f32[2048]{0:T(1024)} %param.18) | copy-start | bytes 24580
  6.5 24.7 %all-gather.15.cloned.1.call-start = ((), (), s32[]{:S(2)}) async-start(), calls=%async_computation.1 | async-start | bytes 1966080 | tf_op jit(solution)/shard_map/all_gather | solution.py:16
  7.3 118.5 %all-gather.17.cloned.1.call-start = ((), (), s32[]{:S(2)}) async-start(), calls=%async_computation.2 | async-start | bytes 6488064 | tf_op jit(solution)/shard_map/all_gather | solution.py:30
  8.0 210.5 %all-gather.19.cloned.1.call-start = ((), (), s32[]{:S(2)}) async-start(), calls=%async_computation.3 | async-start | bytes 6488064 | tf_op jit(solution)/shard_map/all_gather | solution.py:31
  8.7 303.0 %all-gather.21.cloned.1.call-start = ((), (), s32[]{:S(2)}) async-start(), calls=%async_computation.4 | async-start | bytes 6488064 | tf_op jit(solution)/shard_map/all_gather | solution.py:40
  9.3 358.5 %all-gather.35.cloned.1.call-start = ((), (), s32[]{:S(2)}) async-start(), calls=%async_computation.12 | async-start | bytes 7864320 | tf_op jit(solution)/shard_map/all_gather | solution.py:52
  33.1 278.7 %copy-start.2 = (bf16[384,2048]{1,0:T(8,128)(2,1)S(1)}, bf16[384,2048]{1,0:T(8,128)(2,1)}, u32[]{:S(2)}) copy-start(bf16[384,2048]{1,0:T(8,128)(2,1)} %all-gather.15.cloned.1.call-done) | copy-start | bytes 4718596
  323.1 90.9 %all-gather.23.cloned.1.call-start = ((), (), s32[]{:S(2)}) async-start(), calls=%async_computation.5 | async-start | bytes 1769472 | tf_op jit(solution)/shard_map/all_gather | solution.py:72
  323.7 162.3 %all-gather.25.cloned.1.call-start = ((), (), s32[]{:S(2)}) async-start(), calls=%async_computation.6 | async-start | bytes 1769472 | tf_op jit(solution)/shard_map/all_gather | solution.py:73
  324.4 179.3 %all-gather.27.cloned.1.call-start = ((), (), s32[]{:S(2)}) async-start(), calls=%async_computation.7 | async-start | bytes 1769472 | tf_op jit(solution)/shard_map/all_gather | solution.py:105
  325.2 228.6 %all-gather.37.cloned.1.call-start = ((), (), s32[]{:S(2)}) async-start(), calls=%async_computation.13 | async-start | bytes 7864320 | tf_op jit(solution)/shard_map/all_gather | solution.py:52
  373.5 40.5 %copy-start.18 = (f32[2048]{0:T(1024)S(1)}, f32[2048]{0:T(1024)}, u32[]{:S(2)}) copy-start(f32[2048]{0:T(1024)} %param.22) | copy-start | bytes 24580
  375.8 40.7 %copy-start.14 = (f32[384]{0:T(512)}, f32[384]{0:T(512)S(1)}, u32[]{:S(2)}) copy-start(f32[384]{0:T(512)S(1)} %add_rsqrt_fusion.1) | copy-start | bytes 4612
  466.2 12.1 %copy-start.7 = (f32[5,384]{1,0:T(8,128)S(1)}, f32[5,384]{1,0:T(8,128)}, u32[]{:S(2)}) copy-start(f32[5,384]{1,0:T(8,128)} %slice.268) | copy-start | bytes 23044
  483.9 19.8 %copy-start.15 = (f32[384]{0:T(512)S(1)}, f32[384]{0:T(512)}, u32[]{:S(2)}) copy-start(f32[384]{0:T(512)} %copy-done.14) | copy-start | bytes 4612
  483.9 19.8 %copy-start.19 = (f32[2048]{0:T(1024)S(1)}, f32[2048]{0:T(1024)}, u32[]{:S(2)}) copy-start(f32[2048]{0:T(1024)} %param.22) | copy-start | bytes 24580
  509.1 139.1 %all-gather.29.cloned.1.call-start = ((), (), s32[]{:S(2)}) async-start(), calls=%async_computation.8 | async-start | bytes 6488064 | tf_op jit(solution)/shard_map/all_gather | solution.py:30
  509.7 231.2 %all-gather.31.cloned.1.call-start = ((), (), s32[]{:S(2)}) async-start(), calls=%async_computation.9 | async-start | bytes 6488064 | tf_op jit(solution)/shard_map/all_gather | solution.py:31
  510.4 323.7 %all-gather.33.cloned.1.call-start = ((), (), s32[]{:S(2)}) async-start(), calls=%async_computation.10 | async-start | bytes 6488064 | tf_op jit(solution)/shard_map/all_gather | solution.py:40
  511.0 360.7 %reduce-scatter.2.cloned.1.call-start = ((), (), s32[]{:S(2)}) async-start(), calls=%async_computation.11 | async-start | bytes 1966080 | tf_op jit(solution)/shard_map/reduce_scatter | solution.py:46
  558.0 90.2 %copy-start.20 = (f32[2048]{0:T(1024)S(1)}, f32[2048]{0:T(1024)}, u32[]{:S(2)}) copy-start(f32[2048]{0:T(1024)} %param.30) | copy-start | bytes 24580
  648.1 186.0 %copy-start.3 = (bf16[384,2048]{1,0:T(8,128)(2,1)S(1)}, bf16[384,2048]{1,0:T(8,128)(2,1)}, u32[]{:S(2)}) copy-start(bf16[384,2048]{1,0:T(8,128)(2,1)} %get-tuple-element.10) | copy-start | bytes 4718596
  834.1 39.5 %copy-start.1 = (bf16[6,64,64]{2,1,0:T(8,128)(2,1)S(1)}, bf16[6,64,64]{2,1,0:T(8,128)(2,1)}, u32[]{:S(2)}) copy-start(bf16[6,64,64]{2,1,0:T(8,128)(2,1)} %param.26) | copy-start | bytes 147460
  (10 other events, 58.3 us)
Sparse Core Ops, SparseCore 0:
  8.9 22.3 all-gather.14
  33.5 92.3 all-gather.16
  128.0 90.4 all-gather.18
  220.4 91.2 all-gather.20
  323.2 44.5 all-gather.34
  369.8 44.1 all-gather.22
  416.2 42.5 all-gather.24
  460.9 42.7 all-gather.26
  509.2 44.5 all-gather.36
  555.8 92.3 all-gather.28
  650.3 90.4 all-gather.30
  742.8 91.2 all-gather.32
  845.5 26.1 reduce-scatter.1
